TPU v7x, 32 devices: a whole 2x2x4 slice. The times are simulated.
32 devices in a mesh: ep: 8 (over z, x), tp: 4 (over y, core).
Axes of the slice: x: 2, y: 2, z: 4, core: 2. Of those that a mesh axis runs over, the one named last changes fastest.
Arguments:
- mixer_query: bfloat16 [2048, 2048], P('ep', 'tp'), may hold values from -6 to 6
- mixer_forget: bfloat16 [2048, 2048], P('ep', 'tp'), may hold values from -5.5 to 5.5
- mixer_value: bfloat16 [2048, 2048], P('ep', 'tp'), may hold values from -6 to 6
- mixer_gate: bfloat16 [2048, 2048], P('ep', 'tp'), may hold values from -6 to 6
- forget_floor: float32 [2048], P('tp'), may hold values from 0.88 to 1
- head_gain: float32 [128], replicated, may hold values from 0.1 to 1.9
- mixer_proj: bfloat16 [2048, 2048], P(None, 'tp'), may hold values from -0.125 to 0.125
- expert_tokens: bfloat16 [1024, 2048], P('ep'), may hold values from -6 to 6
- expert_gain: float32 [2048], replicated, may hold values from 0.1 to 1.9
- routes: int32 [1024, 2], P('ep'), may hold values from 0 to 7, as said below
- group_logits: float32 [1024, 4], P('ep'), may hold values from -6 to 6
- choice_logits: float32 [1024, 2], P('ep'), may hold values from -6 to 6
- w_gate: bfloat16 [8, 2048, 2048], P('ep', None, 'tp'), may hold values from -0.125 to 0.125
- w_up: bfloat16 [8, 2048, 2048], P('ep', None, 'tp'), may hold values from -0.125 to 0.125
- w_down: bfloat16 [8, 2048, 2048], P('ep', None, 'tp'), may hold values from -0.125 to 0.125
Outputs:
- mixer_out: bfloat16 [2048, 2048], P('ep', 'tp')
- expert_out: bfloat16 [1024, 2048], P('ep', 'tp')
Inputs may be any that keep to these rules, and one draw needn't show every extreme that they name: `routes`: in each aligned block of 128 rows (the rows of one index of ep) no expert is named by more than 64 rows, and some expert reaches that bound in every block; the 2 experts of a row differ and lie in the same group.
All inputs are finite; a program needn't handle non-finite values.
Results may differ from a plain program's by a relative error of at most 0.01.
Values may be sent and summed in bfloat16 or wider, within the bound.
A program may use at most 64 MiB of HBM per device.

v0:
```python
import jax
import jax.numpy as jnp
from jax import lax
from jax.sharding import PartitionSpec as P

KEYDIM = 128
VDIM = 128
GROUPS = 4
TOPK = 2
BLOCK = 64


norm_eps = 1e-06
highest_precision = lax.Precision.HIGHEST


def entering(shard, axis, join, neutral):
    place = lax.axis_index(axis)
    gathered = jax.tree.map(
        lambda a, kind: lax.all_gather(a.astype(kind), axis), shard, (jnp.bfloat16, jnp.bfloat16)
    )
    state = jax.tree.map(lambda a, e: jnp.zeros_like(a) + jnp.asarray(e, a.dtype), shard, neutral)

    def one(lap, state):
        return join(
            state,
            jax.tree.map(
                lambda a, own: lax.dynamic_index_in_dim(a, lap, 0, False).astype(own.dtype),
                gathered,
                shard,
            ),
        )

    return lax.fori_loop(0, place, one, state)


def rms_scale(features, gain_vec):
    return (
        features
        * lax.rsqrt(jnp.mean(features * features, axis=-1, keepdims=True) + norm_eps)
        * gain_vec
    )


def block_terms(query_block, input_block, log_blk, value_block, carried_state):
    cumulative_log = jnp.cumsum(log_blk, axis=0)
    between_block_term = jnp.einsum(
        "zug,ugr->zur",
        query_block * jnp.exp(cumulative_log),
        carried_state,
        precision=highest_precision,
    )
    causal = jnp.tril(jnp.ones((query_block.shape[0], query_block.shape[0]), dtype=bool))[
        :, :, None, None
    ]
    differ = cumulative_log[:, None] - cumulative_log[None, :]
    decays = jnp.exp(jnp.where(causal, differ, -jnp.inf))
    scores = jnp.sum(query_block[:, None] * input_block[None, :] * decays, axis=-1)
    result = between_block_term + jnp.einsum(
        "tsh,shv->thv", scores, value_block, precision=highest_precision
    )
    ending_log_decay = cumulative_log[-1]
    updated_state = jnp.exp(ending_log_decay)[..., None] * carried_state + jnp.einsum(
        "twa,twr->war",
        input_block * jnp.exp(ending_log_decay[None] - cumulative_log),
        value_block,
        precision=highest_precision,
    )
    return (updated_state, result, cumulative_log)


def mixer_local(
    mixer_query, mixer_forget, mixer_value, mixer_gate, forget_floor, head_gain, mixer_proj
):
    length = mixer_query.shape[0]
    heads_local = mixer_query.shape[1] // KEYDIM
    blocks = length // BLOCK

    def split_blocks(source_array, last_width):
        return source_array.reshape(blocks, BLOCK, heads_local, last_width)

    queries = jax.nn.silu(mixer_query.astype(jnp.float32))
    input_rates = (1.0 - forget_floor) * jax.nn.sigmoid(-mixer_forget.astype(jnp.float32))
    log_forget = jnp.log1p(-input_rates)
    value_rows = mixer_value.astype(jnp.float32)

    def advance(carry_pair, block_inputs):
        carried_state, offset_log = carry_pair
        query_block, input_block, value_block, log_blk = block_inputs
        updated_state, result, cumulative_log = block_terms(
            query_block, input_block, log_blk, value_block, carried_state
        )
        scaled_values = query_block * jnp.exp(cumulative_log + offset_log[None])
        return ((updated_state, offset_log + cumulative_log[-1]), (result, scaled_values))

    initial = (
        jnp.zeros((heads_local, KEYDIM, VDIM), jnp.float32),
        jnp.zeros((heads_local, KEYDIM), jnp.float32),
    )
    (local_state, total_log), (output_rows, scaled_values) = lax.scan(
        advance,
        initial,
        (
            split_blocks(queries, KEYDIM),
            split_blocks(input_rates, KEYDIM),
            split_blocks(value_rows, VDIM),
            split_blocks(log_forget, KEYDIM),
        ),
    )

    def combine(earlier, later):
        return (earlier[0] * later[0], later[0][..., None] * earlier[1] + later[1])

    identity = (jnp.ones_like(total_log), jnp.zeros_like(local_state))
    incoming_state = entering((jnp.exp(total_log), local_state), "ep", combine, identity)
    output_rows = output_rows + jnp.einsum(
        "qsfa,fap->qsfp", scaled_values, incoming_state[1], precision=highest_precision
    )
    output_rows = output_rows.reshape(length, heads_local, VDIM)
    gate_act = jax.nn.silu(mixer_gate.astype(jnp.float32)).reshape(length, heads_local, VDIM)
    gated_out = rms_scale(output_rows, head_gain) * gate_act
    mixed_heads = gated_out.reshape(length, heads_local * VDIM).astype(jnp.bfloat16)
    summed = jnp.dot(
        lax.all_gather(mixed_heads, "tp", axis=1, tiled=True),
        mixer_proj,
        preferred_element_type=jnp.float32,
    )
    return summed.astype(jnp.bfloat16)


def gate_weights(routes, group_logits, choice_logits, group_size):
    group_exp = jnp.exp(group_logits)
    group_prob = group_exp / jnp.sum(group_exp, axis=-1, keepdims=True)
    groups_of = routes // group_size
    member = (groups_of[..., None] == jnp.arange(GROUPS, dtype=jnp.int32)).astype(jnp.float32)
    picked_prob = jnp.sum(member * group_prob[:, None, :], axis=-1)
    choice_exp = jnp.exp(choice_logits)
    together = (groups_of[:, :, None] == groups_of[:, None, :]).astype(jnp.float32)
    within = jnp.sum(together * choice_exp[:, None, :], axis=-1)
    return picked_prob * choice_exp / within


def finish(gate_pre, up_pre, down_local, sources, slot_count):
    hidden = (jax.nn.silu(gate_pre) * up_pre).astype(jnp.bfloat16)
    summed = jnp.dot(
        lax.all_gather(hidden, "tp", axis=1, tiled=True),
        down_local,
        preferred_element_type=jnp.float32,
    )
    shaped = summed.astype(jnp.bfloat16).reshape(sources, slot_count, down_local.shape[1])
    return lax.all_to_all(shaped, "ep", split_axis=0, concat_axis=0, tiled=True)


def expert_local(
    expert_tokens, expert_gain, routes, group_logits, choice_logits, w_gate, w_up, w_down
):
    count_rows, model_width = expert_tokens.shape
    experts_all = lax.axis_size("ep")
    capacity = 2 * TOPK * count_rows // experts_all
    normed = rms_scale(expert_tokens.astype(jnp.float32), expert_gain).astype(jnp.bfloat16)
    weights = gate_weights(routes, group_logits, choice_logits, experts_all // GROUPS)
    flat_routes = routes.reshape(-1)
    onehot = (flat_routes[:, None] == jnp.arange(experts_all, dtype=jnp.int32)).astype(jnp.int32)
    earlier = jnp.cumsum(onehot, axis=0) - onehot
    ranks = jnp.sum(earlier * onehot, axis=-1)
    slot_of = flat_routes * capacity + ranks
    token_ids = jnp.arange(flat_routes.shape[0], dtype=jnp.int32) // TOPK
    token_of = jnp.full((experts_all * capacity,), count_rows, jnp.int32).at[slot_of].set(token_ids)
    padded = jnp.concatenate([normed, jnp.zeros((1, model_width), jnp.bfloat16)], axis=0)
    outgoing = padded[token_of].reshape(experts_all, capacity, model_width)
    gate_local = w_gate[0]
    up_local = w_up[0]
    down_local = w_down[0]
    arrived = lax.all_to_all(outgoing, "ep", split_axis=0, concat_axis=0, tiled=True)
    sources, slot_count, _ = arrived.shape
    flat_in = arrived.reshape(sources * slot_count, model_width)
    gate_pre = jnp.dot(flat_in, gate_local, preferred_element_type=jnp.float32)
    up_pre = jnp.dot(flat_in, up_local, preferred_element_type=jnp.float32)
    came_back = finish(gate_pre, up_pre, down_local, sources, slot_count)
    picked = (
        came_back.reshape(-1, came_back.shape[-1])[slot_of].astype(jnp.float32)
        * weights.reshape(-1)[:, None]
    )
    return jnp.sum(picked.reshape(count_rows, TOPK, -1), axis=1).astype(jnp.bfloat16)


def per_device(
    mixer_query,
    mixer_forget,
    mixer_value,
    mixer_gate,
    forget_floor,
    head_gain,
    mixer_proj,
    expert_tokens,
    expert_gain,
    routes,
    group_logits,
    choice_logits,
    w_gate,
    w_up,
    w_down,
):
    mixer_out = mixer_local(
        mixer_query, mixer_forget, mixer_value, mixer_gate, forget_floor, head_gain, mixer_proj
    )
    expert_out = expert_local(
        expert_tokens, expert_gain, routes, group_logits, choice_logits, w_gate, w_up, w_down
    )
    return (mixer_out, expert_out)


def solution(mesh):
    return jax.shard_map(
        per_device,
        mesh=mesh,
        in_specs=(
            P("ep", "tp"),
            P("ep", "tp"),
            P("ep", "tp"),
            P("ep", "tp"),
            P("tp"),
            P(),
            P(None, "tp"),
            P("ep", None),
            P(),
            P("ep", None),
            P("ep", None),
            P("ep", None),
            P("ep", None, "tp"),
            P("ep", None, "tp"),
            P("ep", None, "tp"),
        ),
        out_specs=(P("ep", "tp"), P("ep", "tp")),
        check_vma=False,
    )
```

profile of v0, /device:TPU:0, one launch (start us, length us, event | category | flops | bytes accessed | tf_op | source)
XLA Modules:
  0.0 168.5 jit_solution(13482604115918556136)
XLA Ops:
  10.3 1.4 scatter_custom_fusion
  11.7 1.2 fusion.33
  13.0 1.2 fusion.35
  14.3 3.3 %gather_fusion = bf16[512,2048]{1,0:T(8,128)(2,1)} fusion(bf16[129,2048]{1,0:T(8,128)(2,1)S(1)} %concatenate.3, s32[1024]{0:T(1024)S(1)} %pad_clamp_fusion.1), kind=kCustom, calls=%fused_computation | custom fusion | bytes 4196352 | tf_op jit(solution)/shard_map/gather | solution.py:170
  17.6 7.4 %all-to-all-start = ((bf16[8,64,2048]{2,1,0:T(8,128)(2,1)}), bf16[8,64,2048]{2,1,0:T(8,128)(2,1)}, u32[]{:S(2)}, u32[]{:S(2)}) async-start(bf16[8,64,2048]{2,1,0:T(8,128)(2,1)} %bitcast.133), calls=%async_computation | async-start | bytes 4194304 | tf_op jit(solution)/shard_map/all_to_all | solution.py:174
  25.1 1.2 divide_multiply_fusion
  28.3 1.1 convert_multiply_fusion.3
  29.6 1.9 %reshape.178 = f32[4,64,4,128]{3,2,1,0:T(4,128)} reshape(bf16[256,512]{1,0:T(8,128)(2,1)} %param.21) | data formatting | bytes 786432 | tf_op jit(solution)/shard_map/reshape | solution.py:80
  31.5 37.6 %while.30 = (s32[]{:T(128)}, f32[4,128,128]{2,1,0:T(8,128)S(1)}, f32[4,128]{1,0:T(4,128)S(1)}, f32[4,64,4,128]{3,1,0,2:T(8,128)}, f32[4,64,4,128]{3,1,0,2:T(8,12...) while((s32[]{:T(128)}, f32[4,128,128]{2,1,0:T(8,128)S(1)}, ...), condition=%wide.region_3.4_spmd.clone, body=%wide.region_0.3_spmd.clone.sunk | while | flops 138826752 | bytes 5011073 | solution.py:100
  32.5 1.0 exponential_multiply_fusion.3
  33.5 3.7 %multiply_reduce_fusion.4 = f32[64,64,4]{1,2,0:T(4,128)S(1)} fusion(f32[64,4,128]{2,0,1:T(8,128)S(1)} %copy.120, f32[64,4,128]{2,1,0:T(4,128)S(1)} %fusion.74, f32[64,4,128]{2,0,1:T(8,128)S(1)} %copy.121, f32[64,4,128]{2,1,0:T(4,128)S(1)} %get-tuple-element.314, pred[64,64]{1,0:T(8,128)(4,1)S(1)} %iota_compare_fusion.5), kind=kLoop, calls=%fused_computation.5.clone.1 | loop fusion | flops 10469376 | bytes 593920 | tf_op jit(solution)/shard_map/while/body/eval_jaxpr/reduce_sum | solution.py:58
  41.8 1.0 exponential_multiply_fusion.3
  42.9 3.7 %multiply_reduce_fusion.4 = f32[64,64,4]{1,2,0:T(4,128)S(1)} fusion(f32[64,4,128]{2,0,1:T(8,128)S(1)} %copy.120, f32[64,4,128]{2,1,0:T(4,128)S(1)} %fusion.74, f32[64,4,128]{2,0,1:T(8,128)S(1)} %copy.121, f32[64,4,128]{2,1,0:T(4,128)S(1)} %get-tuple-element.314, pred[64,64]{1,0:T(8,128)(4,1)S(1)} %iota_compare_fusion.5), kind=kLoop, calls=%fused_computation.5.clone.1 | loop fusion | flops 10469376 | bytes 593920 | tf_op jit(solution)/shard_map/while/body/eval_jaxpr/reduce_sum | solution.py:58
  47.9 1.0 fusion.77
  51.2 1.0 exponential_multiply_fusion.3
  52.3 3.7 %multiply_reduce_fusion.4 = f32[64,64,4]{1,2,0:T(4,128)S(1)} fusion(f32[64,4,128]{2,0,1:T(8,128)S(1)} %copy.120, f32[64,4,128]{2,1,0:T(4,128)S(1)} %fusion.74, f32[64,4,128]{2,0,1:T(8,128)S(1)} %copy.121, f32[64,4,128]{2,1,0:T(4,128)S(1)} %get-tuple-element.314, pred[64,64]{1,0:T(8,128)(4,1)S(1)} %iota_compare_fusion.5), kind=kLoop, calls=%fused_computation.5.clone.1 | loop fusion | flops 10469376 | bytes 593920 | tf_op jit(solution)/shard_map/while/body/eval_jaxpr/reduce_sum | solution.py:58
  60.6 1.0 exponential_multiply_fusion.3
  61.7 3.7 %multiply_reduce_fusion.4 = f32[64,64,4]{1,2,0:T(4,128)S(1)} fusion(f32[64,4,128]{2,0,1:T(8,128)S(1)} %copy.120, f32[64,4,128]{2,1,0:T(4,128)S(1)} %fusion.74, f32[64,4,128]{2,0,1:T(8,128)S(1)} %copy.121, f32[64,4,128]{2,1,0:T(4,128)S(1)} %get-tuple-element.314, pred[64,64]{1,0:T(8,128)(4,1)S(1)} %iota_compare_fusion.5), kind=kLoop, calls=%fused_computation.5.clone.1 | loop fusion | flops 10469376 | bytes 593920 | tf_op jit(solution)/shard_map/while/body/eval_jaxpr/reduce_sum | solution.py:58
  69.8 3.5 %all-to-all-done = bf16[8,64,2048]{2,1,0:T(8,128)(2,1)} async-done(((bf16[8,64,2048]{2,1,0:T(8,128)(2,1)}), bf16[8,64,2048]{2,1,0:T(8,128)(2,1)}, u32[]{:S(2)}, u32[]{:S(2)}) %all-to-all-start) | async-done | bytes 2097184 | tf_op jit(solution)/shard_map/all_to_all | solution.py:174
  73.3 3.0 %fusion.22 = f32[512,512]{1,0:T(8,128)S(1)} fusion(bf16[512,2048]{1,0:T(8,128)(2,1)} %bitcast.15, bf16[1,2048,512]{2,1,0:T(8,128)(2,1)S(1)} %copy-done), kind=kOutput, calls=%fused_computation.42 | convolution fusion | flops 1073741824 | bytes 5242880 | tf_op jit(solution)/shard_map/dot_general | solution.py:177
  76.3 3.7 %fusion.30 = bf16[512,512]{1,0:T(8,128)(2,1)} fusion(bf16[512,2048]{1,0:T(8,128)(2,1)} %bitcast.15, bf16[1,2048,512]{2,1,0:T(8,128)(2,1)S(1)} %copy-done.7, f32[512,512]{1,0:T(8,128)S(1)} %fusion.22), kind=kOutput, calls=%fused_computation.48 | convolution fusion | flops 1075314688 | bytes 5767168 | tf_op jit(solution)/shard_map/dot_general | solution.py:178
  80.2 18.7 %all-gather.2 = bf16[8,4,128]{2,1,0:T(4,128)(2,1)S(1)} all-gather(bf16[1,4,128]{2,1,0:T(4,128)(2,1)S(1)} %fusion.49), channel_id=2, replica_groups=mesh['ep'=8,'tp'=4] {'ep'}, dimensions={0}, use_global_device_ids=true | all-gather | bytes 9216 | tf_op jit(solution)/shard_map/all_gather | solution.py:20
  98.8 12.7 %all-gather.11.cloned.1.call-done = bf16[32,128,128]{2,1,0:T(8,128)(2,1)} async-done(((bf16[4,128,128]{2,1,0:T(8,128)(2,1)}), bf16[32,128,128]{2,1,0:T(8,128)(2,1)}) %all-gather.11.cloned.1.call-update) | async-done | bytes 1048592 | tf_op jit(solution)/shard_map/all_gather | solution.py:20
  111.6 1.7 %fusion.52 = f32[4,128,256]{1,2,0:S(1)} fusion(f32[4,128,128]{2,1,0:T(8,128)S(1)} %get-tuple-element.99, f32[4,128,256]{1,2,0:T(8,128)} %bitcast.138), kind=kOutput, calls=%fused_computation.106 | convolution fusion | flops 201326592 | bytes 1310720
  115.3 19.1 %all-gather.9.cloned.1.call-done = bf16[512,2048]{1,0:T(8,128)(2,1)} async-done(((bf16[512,512]{1,0:T(8,128)(2,1)}), bf16[512,2048]{1,0:T(8,128)(2,1)}) %all-gather.9.cloned.1.call-update) | async-done | bytes 2097168 | tf_op jit(solution)/shard_map/all_gather | solution.py:146
  134.4 4.3 %fusion.27 = bf16[512,512]{1,0:T(8,128)(2,1)} fusion(bf16[512,2048]{1,0:T(8,128)(2,1)} %all-gather.9.cloned.1.call-done, bf16[1,2048,512]{2,1,0:T(8,128)(2,1)} %param.33), kind=kOutput, calls=%fused_computation.47 | convolution fusion | flops 1074003968 | bytes 4718592 | tf_op jit(solution)/shard_map/dot_general | solution.py:145
  138.7 5.5 %all-to-all-start.1 = ((bf16[8,64,512]{2,1,0:T(8,128)(2,1)}), bf16[8,64,512]{2,1,0:T(8,128)(2,1)S(1)}, u32[]{:S(2)}, u32[]{:S(2)}) async-start(bf16[8,64,512]{2,1,0:T(8,128)(2,1)} %bitcast.19), calls=%async_computation.1 | async-start | bytes 1048576 | tf_op jit(solution)/shard_map/all_to_all | solution.py:151
  144.4 8.9 %all-gather.7.cloned.1.call-done = bf16[256,2048]{1,0:T(8,128)(2,1)} async-done(((bf16[256,512]{1,0:T(8,128)(2,1)}), bf16[256,2048]{1,0:T(8,128)(2,1)}) %all-gather.7.cloned.1.call-update) | async-done | bytes 1048592 | tf_op jit(solution)/shard_map/all_gather | solution.py:124
  153.3 3.3 %convolution_convert_fusion = bf16[256,512]{1,0:T(8,128)(2,1)} fusion(bf16[256,2048]{1,0:T(8,128)(2,1)} %all-gather.7.cloned.1.call-done, bf16[2048,512]{1,0:T(8,128)(2,1)} %param.25), kind=kOutput, calls=%fused_computation.49 | convolution fusion | flops 537001984 | bytes 3407872 | tf_op jit(solution)/shard_map/dot_general | solution.py:123
  156.7 2.4 %all-to-all-done.1 = bf16[8,64,512]{2,1,0:T(8,128)(2,1)S(1)} async-done(((bf16[8,64,512]{2,1,0:T(8,128)(2,1)}), bf16[8,64,512]{2,1,0:T(8,128)(2,1)S(1)}, u32[]{:S(2)}, u32[]{:S(2)}) %all-to-all-start.1) | async-done | bytes 524320 | tf_op jit(solution)/shard_map/all_to_all | solution.py:151
  159.1 1.2 gather_fusion.1
  160.6 1.4 multiply_reduce_fusion.1
  (111 shorter events, 26.0 us)
Async XLA Ops:
  7.2 66.2 %copy-start = (bf16[1,2048,512]{2,1,0:T(8,128)(2,1)S(1)}, bf16[1,2048,512]{2,1,0:T(8,128)(2,1)}, u32[]{:S(2)}) copy-start(bf16[1,2048,512]{2,1,0:T(8,128)(2,1)} %param.31) | copy-start | bytes 6291460
  17.6 7.5 %copy-start.5 = (f32[512]{0:T(512)S(1)}, f32[512]{0:T(512)}, u32[]{:S(2)}) copy-start(f32[512]{0:T(512)} %param.23) | copy-start | bytes 6148
  17.6 55.8 %all-to-all-start = ((bf16[8,64,2048]{2,1,0:T(8,128)(2,1)}), bf16[8,64,2048]{2,1,0:T(8,128)(2,1)}, u32[]{:S(2)}, u32[]{:S(2)}) async-start(bf16[8,64,2048]{2,1,0:T(8,128)(2,1)} %bitcast.133), calls=%async_computation | async-start | bytes 4194304 | tf_op jit(solution)/shard_map/all_to_all | solution.py:174
  25.0 86.6 %all-gather.11.cloned.1.call-start = ((), (), s32[]{:S(2)}) async-start(), calls=%async_computation.4 | async-start | bytes 1179648 | tf_op jit(solution)/shard_map/all_gather | solution.py:20
  69.8 64.7 %all-gather.9.cloned.1.call-start = ((), (), s32[]{:S(2)}) async-start(), calls=%async_computation.3 | async-start | bytes 2621440 | tf_op jit(solution)/shard_map/all_gather | solution.py:146
  73.3 3.0 %copy-start.7 = (bf16[1,2048,512]{2,1,0:T(8,128)(2,1)S(1)}, bf16[1,2048,512]{2,1,0:T(8,128)(2,1)}, u32[]{:S(2)}) copy-start(bf16[1,2048,512]{2,1,0:T(8,128)(2,1)} %param.32) | copy-start | bytes 6291460
  76.3 22.5 %copy-start.6 = (f32[128]{0:T(128)S(1)}, f32[128]{0:T(128)}, u32[]{:S(2)}) copy-start(f32[128]{0:T(128)} %param.24) | copy-start | bytes 1540
  80.1 73.2 %all-gather.7.cloned.1.call-start = ((), (), s32[]{:S(2)}) async-start(), calls=%async_computation.2 | async-start | bytes 1310720 | tf_op jit(solution)/shard_map/all_gather | solution.py:124
  111.6 1.7 %copy-start.1 = (f32[4,64,4,128]{3,1,0,2:T(8,128)S(1)}, f32[4,64,4,128]{3,1,0,2:T(8,128)}, u32[]{:S(2)}) copy-start(f32[4,64,4,128]{3,1,0,2:T(8,128)} %get-tuple-element.96) | copy-start | bytes 1572868
  111.6 2.8 %copy-start.2 = (bf16[256,512]{1,0:T(8,128)(2,1)S(1)}, bf16[256,512]{1,0:T(8,128)(2,1)}, u32[]{:S(2)}) copy-start(bf16[256,512]{1,0:T(8,128)(2,1)} %param.22) | copy-start | bytes 786436
  113.5 1.8 %copy-start.3 = (f32[128,4]{0,1:T(4,128)S(1)}, f32[128,4]{0,1:T(4,128)}, u32[]{:S(2)}) copy-start(f32[128,4]{0,1:T(4,128)} %param.29) | copy-start | bytes 6148
  115.3 28.9 %copy-start.4 = (f32[128,2]{0,1:T(2,128)S(1)}, f32[128,2]{0,1:T(2,128)}, u32[]{:S(2)}) copy-start(f32[128,2]{0,1:T(2,128)} %param.30) | copy-start | bytes 3076
  138.7 20.4 %all-to-all-start.1 = ((bf16[8,64,512]{2,1,0:T(8,128)(2,1)}), bf16[8,64,512]{2,1,0:T(8,128)(2,1)S(1)}, u32[]{:S(2)}, u32[]{:S(2)}) async-start(bf16[8,64,512]{2,1,0:T(8,128)(2,1)} %bitcast.19), calls=%async_computation.1 | async-start | bytes 1048576 | tf_op jit(solution)/shard_map/all_to_all | solution.py:151
Sparse Core Ops, SparseCore 0:
  69.9 41.6 all-gather.10
  113.1 21.2 all-gather.8
  136.6 16.7 all-gather.6
where the time goes:
time: 169 us; the launch traced here: 168 us
  waiting for transfers between devices  46.7 us (28%)
  other arithmetic  36.4 us (22%)
  matrix products  23.7 us (14%)
  blocking collectives  18.7 us (11%)
  local copies, waits for them, and re-layouts  15.7 us (9%)
  between operations  14 us (8%)
  starting transfers between devices  13 us (8%)
    all_gather x1, waiting for transfers between devices, finish(): lax.all_gather(hidden, 'tp', axis=1, tiled=True)  19.1 us
    all_gather x1, blocking collectives, entering(): lax.all_gather(a.astype(kind), axis)  18.7 us
    reduce_sum x4, other arithmetic, block_terms(): jnp.sum(query_block[:, None] * input_block[None, :] * decays, axis=-1)  14.9 us
    all_gather x1, waiting for transfers between devices, entering(): lax.all_gather(a.astype(kind), axis)  12.7 us
    all_gather x1, waiting for transfers between devices, mixer_local(): lax.all_gather(mixed_heads, 'tp', axis=1, tiled=True)  8.91 us
    all_to_all x1, starting transfers between devices, expert_local(): lax.all_to_all(outgoing, 'ep', split_axis=0, concat_axis=0, tiled=True)  7.41 us
    all_to_all x1, starting transfers between devices, finish(): return lax.all_to_all(shaped, 'ep', split_axis=0, concat_axis=0, tiled=True)  5.51 us
    dot_general x1, matrix products, finish(): jnp.dot(lax.all_gather(hidden, 'tp', axis=1, tiled=True), down_local, pre...  4.26 us
  transfers between devices with their start and end apart: 5, of which 5 were waited for; matrix products, arithmetic and copies ran while one was open for 37% of the time, Pallas kernels for 0%

commit v1 on v0

v1 whole, which is shorter than its diff:
```python
import functools

import jax
import jax.numpy as jnp
from jax import lax
from jax.experimental import pallas as pl
from jax.experimental.pallas import tpu as pltpu
from jax.sharding import PartitionSpec as P

KEYDIM = 128
GROUPS = 4
TOPK = 2
CORES = 2
BATCHES = 2
norm_eps = 1e-06
MESH = pl.DeviceIdType.MESH
f32 = jnp.float32
bf16 = jnp.bfloat16


def mm(a, b):
    return jnp.dot(a, b, preferred_element_type=f32)


def mm_nt(a, b):
    return lax.dot_general(a, b, (((1,), (1,)), ((), ())), preferred_element_type=f32)


def mm_tn(a, b):
    return lax.dot_general(a, b, (((0,), (0,)), ((), ())), preferred_element_type=f32)


def sigmoid(v):
    return 1.0 / (1.0 + jnp.exp(-v))


class Gather:
    def __init__(self, buf, width, tall, ranks, sems):
        self.buf, self.width, self.tall = buf, width, tall
        self.t, self.m = ranks
        self.y, self.c, self.ys = self.t // CORES, self.t % CORES, self.m // CORES
        self.ds, self.dr, self.ps, self.pr = sems
        self.sent = []

    def place(self, y, c, k):
        t = y * CORES + c
        cols = pl.ds(pl.multiple_of(t * self.width, self.width), self.width)
        return self.buf.at[pl.ds(k * self.tall, self.tall), cols]

    def direct(self, dy, k, y):
        ref = self.place(y, self.c, k)
        to = lax.rem(self.y + dy, self.ys) * CORES + self.c
        return pltpu.make_async_remote_copy(
            src_ref=ref, dst_ref=ref, send_sem=self.ds.at[dy - 1, k], recv_sem=self.dr.at[dy - 1, k],
            device_id={"tp": to}, device_id_type=MESH,
        )

    def partner(self, dy, k, c):
        ref = self.place(lax.rem(self.y - dy + self.ys, self.ys), c, k)
        return pltpu.make_async_remote_copy(
            src_ref=ref, dst_ref=ref, send_sem=self.ps.at[dy, k], recv_sem=self.pr.at[dy, k],
            device_id={"tp": self.y * CORES + 1 - self.c}, device_id_type=MESH,
        )

    def go(self, copy):
        copy.start()
        self.sent.append(copy)

    def start(self, k):
        for dy in range(1, self.ys):
            self.go(self.direct(dy, k, self.y))
        self.go(self.partner(0, k, self.c))

    def relay(self, k):
        for dy in range(1, self.ys):
            self.direct(dy, k, lax.rem(self.y - dy + self.ys, self.ys)).wait_recv()
            self.go(self.partner(dy, k, self.c))

    def finish(self, k):
        for dy in range(self.ys):
            self.partner(dy, k, 1 - self.c).wait_recv()

    def drain(self):
        for copy in self.sent:
            copy.wait_send()


def step_kernel(
    n, m, cap,
    q_hbm, f_hbm, v_hbm, g_hbm, floor_ref, hgain_ref, proj_hbm, tok_ref, egain_ref,
    routes_ref, glog_ref, clog_ref, wg_hbm, wu_hbm, wd_hbm,
    mix_out, exp_out,
    q_ref, f_ref, v_ref, g_ref, proj_ref, wg_ref, wu_ref, wd_ref,
    pick0, pick1, slots, xbuf, hbuf, ybuf, rbuf, mbuf, qs_ref, oi_ref,
    s_send, s_recv, d_send, d_recv,
    local_sem, x_s, x_r, r_s, r_r, st_s, st_r,
    xg0, xg1, xg2, xg3, hg0, hg1, hg2, hg3, mg0, mg1, mg2, mg3,
):
    me = lax.axis_index("ep")
    t = lax.axis_index("tp")
    ys = m // CORES
    tokens, width = tok_ref.shape
    wx = width // m
    length, wk = q_ref.shape
    heads = wk // KEYDIM
    wf = wg_ref.shape[1]
    wo = wd_ref.shape[1]
    per = n // BATCHES
    rows_b = per * cap

    def at_ep(k):
        return lax.rem(me + k + n, n)

    loads = []
    pairs = (
        (q_hbm, q_ref), (f_hbm, f_ref), (v_hbm, v_ref), (g_hbm, g_ref),
        (wg_hbm.at[0], wg_ref), (wu_hbm.at[0], wu_ref), (wd_hbm.at[0], wd_ref), (proj_hbm, proj_ref),
    )
    for i, (src, dst) in enumerate(pairs):
        copy = pltpu.make_async_copy(src, dst, local_sem.at[i])
        copy.start()
        loads.append(copy)

    barrier = pltpu.get_barrier_semaphore()
    for k in range(1, n):
        pl.semaphore_signal(barrier, inc=1, device_id={"ep": at_ep(k)}, device_id_type=MESH)
    y, c = t // CORES, t % CORES
    for dy in range(1, ys):
        pl.semaphore_signal(
            barrier, inc=1, device_id={"tp": lax.rem(y + dy, ys) * CORES + c}, device_id_type=MESH
        )
    pl.semaphore_signal(barrier, inc=1, device_id={"tp": y * CORES + 1 - c}, device_id_type=MESH)

    gap = routes_ref[...] - me
    rel = jnp.where(gap < 0, gap + n, gap)
    expert = lax.broadcasted_iota(jnp.int32, (n, tokens), 0)
    is0 = (rel[0:1] == expert).astype(f32)
    is1 = (rel[1:2] == expert).astype(f32)
    before = (
        lax.broadcasted_iota(jnp.int32, (tokens, tokens), 0)
        < lax.broadcasted_iota(jnp.int32, (tokens, tokens), 1)
    ).astype(f32).astype(bf16)
    ranks = mm((is0 + is1).astype(bf16), before)
    slot0 = rel[0:1].astype(f32) * cap + jnp.sum(is0 * ranks, axis=0, keepdims=True)
    slot1 = rel[1:2].astype(f32) * cap + jnp.sum(is1 * ranks, axis=0, keepdims=True)
    slot_ids = lax.broadcasted_iota(jnp.int32, (n * cap, tokens), 0).astype(f32)
    one0 = (slot_ids == slot0).astype(f32)
    one1 = (slot_ids == slot1).astype(f32)
    pick0[...] = one0.astype(bf16)
    pick1[...] = one1.astype(bf16)
    full = tok_ref[...].astype(f32)
    scale = lax.rsqrt(jnp.mean(full * full, axis=-1, keepdims=True) + norm_eps)
    own_cols = pl.ds(pl.multiple_of(t * wx, wx), wx)
    normed = (tok_ref[:, own_cols].astype(f32) * scale * egain_ref[:, own_cols]).astype(bf16)
    slots[...] = mm((one0 + one1).astype(bf16), normed).astype(bf16)
    xbuf[0:cap, own_cols] = slots[0:cap, :]

    pl.semaphore_wait(barrier, (n - 1) + (ys - 1) + 1)

    def x_copy(k):
        return pltpu.make_async_remote_copy(
            src_ref=slots.at[pl.ds(k * cap, cap), :], dst_ref=xbuf.at[pl.ds(k * cap, cap), own_cols],
            send_sem=x_s.at[k - 1], recv_sem=x_r.at[k - 1],
            device_id={"ep": at_ep(k)}, device_id_type=MESH,
        )

    for k in range(1, n):
        x_copy(k).start()
    gx = Gather(xbuf, wx, cap, (t, m), (xg0, xg1, xg2, xg3))
    gx.start(0)

    for i in range(3):
        loads[i].wait()
    rates = (1.0 - floor_ref[...]) * sigmoid(-f_ref[...].astype(f32))
    log_forget = jnp.log(1.0 - rates)
    row = lax.broadcasted_iota(jnp.int32, (length, length), 0)
    col = lax.broadcasted_iota(jnp.int32, (length, length), 1)
    causal = row >= col
    upto = causal.astype(f32).astype(bf16)
    high = log_forget.astype(bf16)
    low = (log_forget - high.astype(f32)).astype(bf16)
    cumulative = mm(upto, high) + mm(upto, low)
    last = cumulative[length - 1 : length, :]
    pre = q_ref[...].astype(f32)
    scaled_q = (pre * sigmoid(pre) * jnp.exp(cumulative)).astype(bf16)
    qs_ref[...] = scaled_q
    scaled_k = (rates * jnp.exp(-cumulative)).astype(bf16)
    tail_k = (rates * jnp.exp(last - cumulative)).astype(bf16)
    states = []
    for h in range(heads):
        cols = slice(h * KEYDIM, (h + 1) * KEYDIM)
        values = v_ref[:, cols]
        scores = jnp.where(causal, mm_nt(scaled_q[:, cols], scaled_k[:, cols]), 0.0).astype(bf16)
        oi_ref[:, cols] = mm(scores, values)
        states.append(mm_tn(values, tail_k[:, cols]))
    win_s = jnp.concatenate(states, axis=1) if heads > 1 else states[0]
    win_a = jnp.exp(last)
    pre_s = jnp.zeros_like(win_s)
    pre_a = jnp.ones_like(win_a)

    def state_copies(r):
        to = {"ep": at_ep(1 << r)}
        return (
            pltpu.make_async_remote_copy(
                src_ref=s_send.at[r], dst_ref=s_recv.at[r], send_sem=st_s.at[0, r], recv_sem=st_r.at[0, r],
                device_id=to, device_id_type=MESH,
            ),
            pltpu.make_async_remote_copy(
                src_ref=d_send.at[r], dst_ref=d_recv.at[r], send_sem=st_s.at[1, r], recv_sem=st_r.at[1, r],
                device_id=to, device_id_type=MESH,
            ),
        )

    rounds = (n - 1).bit_length()

    def state_send(r, a, s):
        s_send[r] = s.astype(bf16)
        d_send[r] = jnp.broadcast_to(a, d_send.shape[1:])

        @pl.when(me + (1 << r) < n)
        def _():
            for copy in state_copies(r):
                copy.start()

    def state_take(r, pre_pair, win_pair):
        @pl.when(me >= (1 << r))
        def _():
            for copy in state_copies(r):
                copy.wait_recv()

        @pl.when(me < (1 << r))
        def _():
            s_recv[r] = jnp.zeros(s_recv.shape[1:], bf16)
            d_recv[r] = jnp.ones(d_recv.shape[1:], f32)

        got_s = s_recv[r].astype(f32)
        got_a = d_recv[r, 0:1, :]
        (pa, ps), (wa, ws) = pre_pair, win_pair
        return (pa * got_a, pa * got_s + ps), (wa * got_a, wa * got_s + ws)

    prefix, window = (pre_a, pre_s), (win_a, win_s)
    state_send(0, *window)

    def forward(k):
        x_copy(k).wait_recv()
        gx.start(k)

    for k in range(1, per):
        forward(k)
        gx.relay(k - 1)
    done = 0
    prefix, window = state_take(0, prefix, window)
    done = 1
    if done < rounds:
        state_send(1, *window)
    for k in range(per, n):
        forward(k)
        if k == per:
            gx.relay(k - 1)
    loads[4].wait()
    loads[5].wait()
    gh = Gather(hbuf, wf, rows_b, (t, m), (hg0, hg1, hg2, hg3))
    own_hidden = pl.ds(pl.multiple_of(t * wf, wf), wf)

    def experts_in(b):
        for k in range(b * per, (b + 1) * per):
            gx.finish(k)
        span = slice(b * rows_b, (b + 1) * rows_b)
        x = xbuf[span, :]
        gate = mm(x, wg_ref[...])
        up = mm(x, wu_ref[...])
        hbuf[span, own_hidden] = (gate * sigmoid(gate) * up).astype(bf16)
        gh.start(b)

    for b in range(BATCHES):
        if b > 0:
            for k in range(b * per, (b + 1) * per):
                gx.relay(k)
        experts_in(b)
        if done < rounds:
            prefix, window = state_take(done, prefix, window)
            done += 1
            if done < rounds:
                state_send(done, *window)
    while done < rounds:
        prefix, window = state_take(done, prefix, window)
        done += 1
        if done < rounds:
            state_send(done, *window)

    loads[3].wait()
    entering = prefix[1].astype(bf16)
    gm = Gather(mbuf, wk, length, (t, m), (mg0, mg1, mg2, mg3))
    for h in range(heads):
        cols = slice(h * KEYDIM, (h + 1) * KEYDIM)
        out = oi_ref[:, cols] + mm_nt(qs_ref[:, cols], entering[:, cols])
        gate = g_ref[:, cols].astype(f32)
        out = out * lax.rsqrt(jnp.mean(out * out, axis=-1, keepdims=True) + norm_eps)
        out = out * hgain_ref[...] * (gate * sigmoid(gate))
        place = pl.ds(pl.multiple_of(t * wk + h * KEYDIM, KEYDIM), KEYDIM)
        mbuf[:, place] = out.astype(bf16)
    gm.start(0)

    def r_copy(k):
        span = pl.ds(k * cap, cap)
        return pltpu.make_async_remote_copy(
            src_ref=ybuf.at[span, :], dst_ref=rbuf.at[span, :],
            send_sem=r_s.at[k - 1], recv_sem=r_r.at[k - 1],
            device_id={"ep": at_ep(-k)}, device_id_type=MESH,
        )

    loads[6].wait()
    for b in range(BATCHES):
        gh.relay(b)
        gh.finish(b)
        span = slice(b * rows_b, (b + 1) * rows_b)
        ybuf[span, :] = mm(hbuf[span, :], wd_ref[...]).astype(bf16)
        for k in range(max(1, b * per), (b + 1) * per):
            r_copy(k).start()

    gm.relay(0)
    gm.finish(0)
    loads[7].wait()
    mix_out[...] = mm(mbuf[...], proj_ref[...]).astype(bf16)

    group_exp = jnp.exp(glog_ref[...])
    group_prob = group_exp / jnp.sum(group_exp, axis=0, keepdims=True)
    size = n // GROUPS
    low_id = lax.broadcasted_iota(jnp.int32, (GROUPS, tokens), 0) * size
    routes = routes_ref[...]
    in0 = ((routes[0:1] >= low_id) & (routes[0:1] < low_id + size)).astype(f32)
    in1 = ((routes[1:2] >= low_id) & (routes[1:2] < low_id + size)).astype(f32)
    same = jnp.sum(in0 * in1, axis=0, keepdims=True)
    choice_exp = jnp.exp(clog_ref[...])
    ce0, ce1 = choice_exp[0:1], choice_exp[1:2]
    w0 = jnp.sum(in0 * group_prob, axis=0, keepdims=True) * ce0 / (ce0 + same * ce1)
    w1 = jnp.sum(in1 * group_prob, axis=0, keepdims=True) * ce1 / (ce1 + same * ce0)
    w0 = jnp.transpose(jnp.broadcast_to(w0, (128, tokens)))[:, 0:1]
    w1 = jnp.transpose(jnp.broadcast_to(w1, (128, tokens)))[:, 0:1]

    rbuf[0:cap, :] = ybuf[0:cap, :]
    for k in range(1, n):
        r_copy(k).wait_recv()
    back = rbuf[...]
    exp_out[...] = (w0 * mm_tn(pick0[...], back) + w1 * mm_tn(pick1[...], back)).astype(bf16)

    for k in range(1, n):
        x_copy(k).wait_send()
        r_copy(k).wait_send()
    for r in range(rounds):
        @pl.when(me + (1 << r) < n)
        def _():
            for copy in state_copies(r):
                copy.wait_send()
    gx.drain()
    gh.drain()
    gm.drain()


def per_device(n, m, mq, mf, mv, mg, floor, hgain, proj, tok, egain, routes, glog, clog, wg, wu, wd):
    length, wk = mq.shape
    tokens, width = tok.shape
    wf, wo = wg.shape[2], wd.shape[2]
    cap = 2 * TOPK * tokens // n
    rows = n * cap
    ys = m // CORES
    rounds = (n - 1).bit_length()
    vmem = pl.BlockSpec(memory_space=pltpu.VMEM)
    hbm = pl.BlockSpec(memory_space=pl.ANY)

    def gather_sems(chunks):
        dma = pltpu.SemaphoreType.DMA
        return [dma((ys - 1, chunks)), dma((ys - 1, chunks)), dma((ys, chunks)), dma((ys, chunks))]

    dma = pltpu.SemaphoreType.DMA
    scratch = [
        pltpu.VMEM((length, wk), bf16), pltpu.VMEM((length, wk), bf16),
        pltpu.VMEM((length, wk), bf16), pltpu.VMEM((length, wk), bf16),
        pltpu.VMEM(proj.shape, bf16),
        pltpu.VMEM(wg.shape[1:], bf16), pltpu.VMEM(wu.shape[1:], bf16), pltpu.VMEM(wd.shape[1:], bf16),
        pltpu.VMEM((rows, tokens), bf16), pltpu.VMEM((rows, tokens), bf16),
        pltpu.VMEM((rows, width // m), bf16),
        pltpu.VMEM((rows, width), bf16),
        pltpu.VMEM((rows, wd.shape[1]), bf16),
        pltpu.VMEM((rows, wo), bf16), pltpu.VMEM((rows, wo), bf16),
        pltpu.VMEM((length, proj.shape[0]), bf16),
        pltpu.VMEM((length, wk), bf16), pltpu.VMEM((length, wk), f32),
        pltpu.VMEM((rounds, KEYDIM, wk), bf16), pltpu.VMEM((rounds, KEYDIM, wk), bf16),
        pltpu.VMEM((rounds, 8, wk), f32), pltpu.VMEM((rounds, 8, wk), f32),
        dma((8,)), dma((n - 1,)), dma((n - 1,)), dma((n - 1,)), dma((n - 1,)),
        dma((2, rounds)), dma((2, rounds)),
    ] + gather_sems(n) + gather_sems(BATCHES) + gather_sems(1)
    return pl.pallas_call(
        functools.partial(step_kernel, n, m, cap),
        out_shape=(
            jax.ShapeDtypeStruct((length, proj.shape[1]), bf16),
            jax.ShapeDtypeStruct((tokens, wo), bf16),
        ),
        in_specs=[hbm, hbm, hbm, hbm, vmem, vmem, hbm, vmem, vmem, vmem, vmem, vmem, hbm, hbm, hbm],
        out_specs=(vmem, vmem),
        scratch_shapes=scratch,
        compiler_params=pltpu.CompilerParams(
            collective_id=0, has_side_effects=True, vmem_limit_bytes=60 * 1024 * 1024
        ),
    )(
        mq, mf, mv, mg, floor[None, :], hgain[None, :], proj, tok, egain[None, :],
        routes.T, glog.T, clog.T, wg, wu, wd,
    )


def solution(mesh):
    return jax.shard_map(
        functools.partial(per_device, mesh.shape["ep"], mesh.shape["tp"]),
        mesh=mesh,
        in_specs=(
            P("ep", "tp"), P("ep", "tp"), P("ep", "tp"), P("ep", "tp"), P("tp"), P(), P(None, "tp"),
            P("ep", None), P(), P("ep", None), P("ep", None), P("ep", None),
            P("ep", None, "tp"), P("ep", None, "tp"), P("ep", None, "tp"),
        ),
        out_specs=(P("ep", "tp"), P("ep", "tp")),
        check_vma=False,
    )
```

time: 169 us -> 57.8 us (0.34)
  Pallas kernels: 0 us -> 53.7 us
  waiting for transfers between devices: 46.7 us -> 0 us
  other arithmetic: 36.4 us -> 0 us
  matrix products: 23.7 us -> 0 us
  blocking collectives: 18.7 us -> 0 us
  between operations: 14 us -> 0.64 us
  starting transfers between devices: 13 us -> 0 us
  local copies, waits for them, and re-layouts: 15.7 us -> 3.24 us
    pallas_call x0 -> x1, Pallas kernels: none -> 53.7 us  [per_device(): pl.pallas_call(functools.partial(step_kernel, n, m, cap), out_shape=(jax....]
    all_gather x3 -> x0, waiting for transfers between devices: 40.7 us -> none  [the longest x1 19.1 us: finish(): lax.all_gather(hidden, 'tp', axis=1, tiled=True)]
    dot_general x16 -> x0, matrix products: 22 us -> none  [the longest x1 4.26 us: finish(): jnp.dot(lax.all_gather(hidden, 'tp', axis=1, tiled=True), down_local, pre...]
    all_gather x1 -> x0, blocking collectives: 18.7 us -> none  [entering(): lax.all_gather(a.astype(kind), axis)]
    reduce_sum x11 -> x0, other arithmetic: 17.9 us -> none  [the longest x4 14.9 us: block_terms(): jnp.sum(query_block[:, None] * input_block[None, :] * decays, axis=-1)]
    all_to_all x2 -> x0, starting transfers between devices: 12.9 us -> none  [the longest x1 7.41 us: expert_local(): lax.all_to_all(outgoing, 'ep', split_axis=0, concat_axis=0, tiled=True)]
    mul x10 -> x0, other arithmetic: 10.3 us -> none  [the longest x4 4.08 us: block_terms(): query_block * jnp.exp(cumulative_log)]
    all_to_all x2 -> x0, waiting for transfers between devices: 5.94 us -> none  [the longest x1 3.51 us: expert_local(): lax.all_to_all(outgoing, 'ep', split_axis=0, concat_axis=0, tiled=True)]
  transfers between devices with their start and end apart: 5 -> 0, of which waited for: 5 -> 0; matrix products, arithmetic and copies ran while one was open for 37% -> 0% of each run, Pallas kernels for 0% -> 0%
where the time goes in v1:
time: 57.8 us; the launch traced here: 57.6 us
  Pallas kernels  53.7 us (93%)
  local copies, waits for them, and re-layouts  3.24 us (6%)
  between operations  0.64 us (1%)
    pallas_call x1, Pallas kernels, per_device(): pl.pallas_call(functools.partial(step_kernel, n, m, cap), out_shape=(jax....  53.7 us
    unnamed x2, local copies, waits for them, and re-layouts  3.24 us

profile of v1, /device:TPU:0, one launch (start us, length us, event | category | flops | bytes accessed | tf_op | source)
XLA Modules:
  0.0 57.6 jit_solution(2585887285786331485)
XLA Ops:
  0.6 53.7 %shard_map.158 = (bf16[256,512]{1,0:T(8,128)(2,1)}, bf16[128,512]{1,0:T(8,128)(2,1)}) custom-call(bf16[256,512]{1,0:T(8,128)(2,1)} %q_hbm.1, bf16[256,512]{1,0:T(8,128)(2,1)} %f_hbm.1, bf16[256,512]{1,0:T(8,128)(2,1)} %v_hbm.1, bf16[256,512]{1,0:T(8,128)(2,1)} %g_hbm.1, f32[1,512]{1,0:T(1,128)} %bitcast.7, f32[1,128]{1,0:T(1,128)} %bitcast.11, ...), custom_call_target="tpu_custom_call" | custom-call | tf_op jit(solution)/shard_map/pallas_call | solution.py:393
  54.4 1.7 %copy.19 = bf16[256,512]{1,0:T(8,128)(2,1)} copy(bf16[256,512]{1,0:T(8,128)(2,1)} %get-tuple-element.4) | data formatting | bytes 524288
  56.1 1.6 %copy.20 = bf16[128,512]{1,0:T(8,128)(2,1)} copy(bf16[128,512]{1,0:T(8,128)(2,1)} %get-tuple-element.5) | data formatting | bytes 262144
